TPU v7x, 32 devices: a whole 2x2x4 slice. The times are simulated.
32 devices in a mesh: ra: 4 (over z), cb: 4 (over y, x), dp: 2 (over core).
Axes of the slice: x: 2, y: 2, z: 4, core: 2. Of those that a mesh axis runs over, the one named last changes fastest.
Arguments:
- carried: bfloat16 [3072, 4096], P('dp', 'ra'), may hold values from -100 to 100
- branch_in: bfloat16 [3072, 4096], P('dp', 'ra'), may hold values from -12 to 12
- gain_in: float32 [4096], P('ra'), may hold values from 0.1 to 1.9
- bias_in: float32 [4096], P('ra'), may hold values from -1.8 to 1.8
- up_weight: bfloat16 [4096, 16384], P('ra', 'cb'), may hold values from -0.125 to 0.125
- down_weight: bfloat16 [16384, 4096], P('cb', 'ra'), may hold values from -0.046875 to 0.046875
- gain_out: float32 [4096], P('ra'), may hold values from 0.1 to 1.9
- bias_out: float32 [4096], P('ra'), may hold values from -1.8 to 1.8
Outputs:
- layer_out: bfloat16 [3072, 4096], P('dp', 'ra')
All inputs are finite; a program needn't handle non-finite values.
Results may differ from a plain program's by a relative error of at most 0.006.
Values may be sent and summed in bfloat16 or wider, within the bound.
A program may use at most 128 MiB of HBM per device.

v0:
```python
import jax
import jax.numpy as jnp
from jax import lax
from jax.sharding import PartitionSpec as P

residual_scale = 2.0**0.25
norm_eps = 1e-05


def normalize(mixed, totals, squares, width, gain, bias):
    mean = totals[:, None] / width
    spread = squares[:, None] / width - mean * mean
    return (mixed - mean) * lax.rsqrt(spread + norm_eps) * gain + bias


def per_device(carried, branch_in, gain_in, bias_in, up_weight, down_weight, gain_out, bias_out):
    width = carried.shape[1] * lax.axis_size("ra")
    mixed_in = residual_scale * carried.astype(jnp.float32) + branch_in.astype(jnp.float32)
    totals, squares = lax.psum(
        (jnp.sum(mixed_in, axis=1), jnp.sum(mixed_in * mixed_in, axis=1)), "ra"
    )
    normed = normalize(mixed_in, totals, squares, width, gain_in, bias_in).astype(jnp.bfloat16)
    regrouped = lax.all_to_all(up_weight, "ra", split_axis=1, concat_axis=0, tiled=True)
    pre_share = lax.dot_general(
        regrouped,
        lax.all_gather(normed, "ra", axis=1, tiled=True),
        (((0,), (1,)), ((), ())),
        preferred_element_type=jnp.float32,
    )
    hidden_share = jnp.square(jnp.maximum(pre_share, 0.0)).astype(jnp.bfloat16)
    branch_part = lax.dot_general(
        lax.all_gather(hidden_share, "ra", axis=0, tiled=True),
        down_weight,
        (((0,), (0,)), ((), ())),
        preferred_element_type=jnp.float32,
    )
    branch_out = lax.psum(branch_part, "cb")
    mixed_out = residual_scale * normed.astype(jnp.float32) + branch_out
    totals_out, squares_out = lax.psum(
        (jnp.sum(mixed_out, axis=1), jnp.sum(mixed_out * mixed_out, axis=1)), "ra"
    )
    return normalize(mixed_out, totals_out, squares_out, width, gain_out, bias_out).astype(
        jnp.bfloat16
    )


def solution(mesh):
    in_specs = (
        P("dp", "ra"),
        P("dp", "ra"),
        P("ra"),
        P("ra"),
        P("ra", "cb"),
        P("cb", "ra"),
        P("ra"),
        P("ra"),
    )
    out_specs = P("dp", "ra")
    return jax.shard_map(
        per_device, mesh=mesh, in_specs=in_specs, out_specs=out_specs, check_vma=False
    )
```

profile of v0, /device:TPU:0, one launch (start us, length us, event | category | flops | bytes accessed | tf_op | source)
XLA Modules:
  0.0 859.6 jit_solution(17207012379904280185)
XLA Ops:
  6.5 0.0 copy-start.1
  6.5 0.0 copy-start.2
  6.5 0.0 copy-start.3
  6.5 0.0 all-gather.3.cloned.1.call-start
  6.5 4.5 fusion
  11.1 20.5 %all-reduce.1 = (f32[1536]{0:T(1024)S(1)}, f32[1536]{0:T(1024)S(1)}) all-reduce(f32[1536]{0:T(1024)S(1)} %get-tuple-element.8, f32[1536]{0:T(1024)S(1)} %get-tuple-element.7), channel_id=1, replica_groups=mesh['ra'=4,'cb'=4,'dp'=2] {'ra'}, use_global_device_ids=true, to_apply=%region_3.0 | all-reduce | flops 3072 | bytes 24576 | tf_op jit(solution)/shard_map/psum | solution.py:19
  31.6 0.0 copy-done.1
  31.6 0.0 copy-done.2
  31.6 0.0 copy-done.3
  31.6 4.5 add_convert_fusion.1
  36.2 0.0 all-gather.3.cloned.1.call-update
  36.2 0.0 all-gather.5.cloned.1.call-start
  36.2 12.2 %copy.9 = bf16[1024,4096]{0,1:T(8,128)(2,1)} copy(bf16[1024,4096]{1,0:T(8,128)(2,1)} %param.12) | data formatting | bytes 16777216 | tf_op args[4]
  48.5 373.1 %all_to_all.19 = bf16[1024,4,1024]{0,2,1:T(8,128)(2,1)} all-to-all(bf16[1024,4,1024]{0,2,1:T(8,128)(2,1)} %bitcast.10), channel_id=1, replica_groups=mesh['ra'=4,'cb'=4,'dp'=2] {'ra'}, dimensions={1} | all-to-all | bytes 16777216 | tf_op jit(solution)/shard_map/all_to_all | solution.py:23
  421.6 11.4 %copy.10 = bf16[4,1024,1024]{2,1,0:T(8,128)(2,1)} copy(bf16[4,1024,1024]{1,2,0:T(8,128)(2,1)} %bitcast.9) | data formatting | bytes 16777216 | tf_op jit(solution)/shard_map/all_to_all | solution.py:23
  432.9 0.0 all-gather.3.cloned.1.call-done
  432.9 19.2 %fusion.1 = bf16[1024,1536]{0,1:T(8,128)(2,1)} fusion(bf16[1536,4096]{1,0:T(8,128)(2,1)} %all-gather.3.cloned.1.call-done, bf16[4096,1024]{1,0:T(8,128)(2,1)} %bitcast.11), kind=kOutput, calls=%fused_computation.8 | convolution fusion | flops 12889620480 | bytes 24117248 | tf_op jit(solution)/shard_map/dot_general | solution.py:24
  452.1 0.0 all-gather.5.cloned.1.call-update
  452.1 0.2 all-reduce.4.cloned.1.call-start
  452.3 216.9 %all-gather.5.cloned.1.call-done = bf16[4096,1536]{0,1:T(8,128)(2,1)} async-done(((bf16[1024,1536]{0,1:T(8,128)(2,1)}), bf16[4096,1536]{0,1:T(8,128)(2,1)}) %all-gather.5.cloned.1.call-update) | async-done | bytes 12582928 | tf_op jit(solution)/shard_map/all_gather | solution.py:32
  669.2 19.5 %fusion.3 = f32[1536,1024]{1,0:T(8,128)} fusion(bf16[4096,1536]{0,1:T(8,128)(2,1)} %all-gather.5.cloned.1.call-done, bf16[4096,1024]{1,0:T(8,128)(2,1)} %param.13), kind=kOutput, calls=%fused_computation.14 | convolution fusion | flops 12884901888 | bytes 27262976 | tf_op jit(solution)/shard_map/dot_general | solution.py:31
  688.7 0.0 copy-start
  688.7 0.0 all-reduce.4.cloned.1.call-update
  688.8 0.0 copy-start.4
  688.8 0.0 copy-start.5
  688.8 136.5 %all-reduce.4.cloned.1.call-done = f32[1536,1024]{1,0:T(8,128)} async-done(((f32[1536,1024]{1,0:T(8,128)}), f32[1536,1024]{1,0:T(8,128)}) %all-reduce.4.cloned.1.call-update) | async-done | bytes 6291472 | tf_op jit(solution)/shard_map/psum | solution.py:37
  825.3 0.0 copy-done
  825.3 4.1 fusion.2
  829.4 18.7 %all-reduce = (f32[1536]{0:T(1024)S(1)}, f32[1536]{0:T(1024)S(1)}) all-reduce(f32[1536]{0:T(1024)S(1)} %get-tuple-element.6, f32[1536]{0:T(1024)S(1)} %get-tuple-element.5), channel_id=1, replica_groups=mesh['ra'=4,'cb'=4,'dp'=2] {'ra'}, use_global_device_ids=true, to_apply=%region_8.0 | all-reduce | flops 3072 | bytes 24576 | tf_op jit(solution)/shard_map/psum | solution.py:39
  848.1 0.0 copy-done.4
  848.1 0.0 copy-done.5
  848.1 4.9 add_convert_fusion
  (2 shorter events, 0.0 us)
Async XLA Ops:
  6.5 25.1 %copy-start.1 = (bf16[1536,1024]{1,0:T(8,128)(2,1)S(1)}, bf16[1536,1024]{1,0:T(8,128)(2,1)}, u32[]{:S(2)}) copy-start(bf16[1536,1024]{1,0:T(8,128)(2,1)} %param.9) | copy-start | bytes 9437188
  6.5 25.1 %copy-start.2 = (f32[1024]{0:T(1024)S(1)}, f32[1024]{0:T(1024)}, u32[]{:S(2)}) copy-start(f32[1024]{0:T(1024)} %param.11) | copy-start | bytes 12292
  6.5 25.1 %copy-start.3 = (f32[1024]{0:T(1024)S(1)}, f32[1024]{0:T(1024)}, u32[]{:S(2)}) copy-start(f32[1024]{0:T(1024)} %param.10) | copy-start | bytes 12292
  6.5 426.4 %all-gather.3.cloned.1.call-start = ((), (), s32[]{:S(2)}) async-start(), calls=%async_computation.1 | async-start | bytes 15728640 | tf_op jit(solution)/shard_map/all_gather | solution.py:26
  36.2 633.1 %all-gather.5.cloned.1.call-start = ((), (), s32[]{:S(2)}) async-start(), calls=%async_computation.2 | async-start | bytes 15728640 | tf_op jit(solution)/shard_map/all_gather | solution.py:32
  452.1 373.1 %all-reduce.4.cloned.1.call-start = ((), (), s32[]{:S(2)}) async-start(), calls=%async_computation.3 | async-start | bytes 12582912 | tf_op jit(solution)/shard_map/psum | solution.py:37
  688.7 136.5 %copy-start = (bf16[1536,1024]{1,0:T(8,128)(2,1)S(1)}, bf16[1536,1024]{1,0:T(8,128)(2,1)}, u32[]{:S(2)}) copy-start(bf16[1536,1024]{1,0:T(8,128)(2,1)} %add_convert_fusion.1) | copy-start | bytes 9437188
  688.8 159.4 %copy-start.4 = (f32[1024]{0:T(1024)S(1)}, f32[1024]{0:T(1024)}, u32[]{:S(2)}) copy-start(f32[1024]{0:T(1024)} %param.15) | copy-start | bytes 12292
  688.8 159.4 %copy-start.5 = (f32[1024]{0:T(1024)S(1)}, f32[1024]{0:T(1024)}, u32[]{:S(2)}) copy-start(f32[1024]{0:T(1024)} %param.14) | copy-start | bytes 12292
Sparse Core Ops, SparseCore 0:
  36.3 395.6 all-gather.2
  452.2 216.9 all-gather.4
  688.9 136.3 all-reduce.3
where the time goes:
time: 860 us
  blocking collectives  412 us (48%)
  waiting for transfers between devices  353 us (41%)
  matrix products  38.6 us (4%)
  local copies, waits for them, and re-layouts  23.6 us (3%)
  other arithmetic  18.1 us (2%)
  between operations  13.2 us (2%)
    all_to_all x1, blocking collectives, per_device(): lax.all_to_all(up_weight, 'ra', split_axis=1, concat_axis=0, tiled=True)  373 us
    all_gather x1, waiting for transfers between devices, per_device(): lax.all_gather(hidden_share, 'ra', axis=0, tiled=True)  217 us
    psum x1, waiting for transfers between devices, per_device(): branch_out = lax.psum(branch_part, 'cb')  136 us
    psum x1, blocking collectives, per_device(): lax.psum((jnp.sum(mixed_in, axis=1), jnp.sum(mixed_in * mixed_in, axis=1)...  20.5 us
    dot_general x1, matrix products, per_device(): lax.dot_general(lax.all_gather(hidden_share, 'ra', axis=0, tiled=True), d...  19.5 us
    dot_general x1, matrix products, per_device(): lax.dot_general(regrouped, lax.all_gather(normed, 'ra', axis=1, tiled=Tru...  19.2 us
    psum x1, blocking collectives, per_device(): lax.psum((jnp.sum(mixed_out, axis=1), jnp.sum(mixed_out * mixed_out, axis...  18.7 us
  transfers between devices with their start and end apart: 3, of which 2 were waited for; matrix products, arithmetic and copies ran while one was open for 3% of the time, Pallas kernels for 0%

commit v1 on v0

--- a/solution.py
+++ b/solution.py
@@ -34,7 +34,11 @@
         (((0,), (0,)), ((), ())),
         preferred_element_type=jnp.float32,
     )
-    branch_out = lax.psum(branch_part, "cb")
+    branch_out = branch_part
+    for hop in (1, 2):
+        branch_out = branch_out + lax.ppermute(
+            branch_out, "cb", [(dev, dev ^ hop) for dev in range(4)]
+        )
     mixed_out = residual_scale * normed.astype(jnp.float32) + branch_out
     totals_out, squares_out = lax.psum(
         (jnp.sum(mixed_out, axis=1), jnp.sum(mixed_out * mixed_out, axis=1)), "ra"

time: 860 us -> 1010 us (1.17)
  waiting for transfers between devices: 353 us -> 488 us
  local copies, waits for them, and re-layouts: 23.6 us -> 34.3 us
    ppermute x0 -> x2, waiting for transfers between devices: none -> 271 us  [per_device(): lax.ppermute(branch_out, 'cb', [(dev, dev ^ hop) for dev in range(4)])]
    psum x1 -> x0, waiting for transfers between devices: 136 us -> none  [per_device(): branch_out = lax.psum(branch_part, 'cb')]
  transfers between devices with their start and end apart: 3 -> 4, of which waited for: 2 -> 3; matrix products, arithmetic and copies ran while one was open for 3% -> 2% of each run, Pallas kernels for 0% -> 0%
where the time goes in v1:
time: 1010 us; the launch traced here: 1000 us
  waiting for transfers between devices  488 us (48%)
  blocking collectives  409 us (40%)
  matrix products  37.1 us (4%)
  local copies, waits for them, and re-layouts  34.3 us (3%)
  other arithmetic  19.3 us (2%)
  between operations  13.5 us (1%)
    all_to_all x1, blocking collectives, per_device(): lax.all_to_all(up_weight, 'ra', split_axis=1, concat_axis=0, tiled=True)  373 us
    ppermute x2, waiting for transfers between devices, per_device(): lax.ppermute(branch_out, 'cb', [(dev, dev ^ hop) for dev in range(4)])  271 us
    all_gather x1, waiting for transfers between devices, per_device(): lax.all_gather(hidden_share, 'ra', axis=0, tiled=True)  217 us
    psum x1, blocking collectives, per_device(): lax.psum((jnp.sum(mixed_in, axis=1), jnp.sum(mixed_in * mixed_in, axis=1)...  20.5 us
  transfers between devices with their start and end apart: 4, of which 3 were waited for; matrix products, arithmetic and copies ran while one was open for 2% of the time, Pallas kernels for 0%

profile of v1, /device:TPU:0, one launch (start us, length us, event | category | flops | bytes accessed | tf_op | source)
XLA Modules:
  0.0 1005.0 jit_solution(14767584129587551216)
XLA Ops:
  6.5 0.0 all-gather.3.cloned.1.call-start
  6.5 3.2 copy.15
  9.7 0.0 copy-start.1
  9.7 0.0 copy-start.2
  9.7 4.6 copy.16
  14.4 3.3 fusion
  17.7 20.5 %all-reduce.1 = (f32[1536]{0:T(1024)S(1)}, f32[1536]{0:T(1024)S(1)}) all-reduce(f32[1536]{0:T(1024)S(1)} %get-tuple-element.8, f32[1536]{0:T(1024)S(1)} %get-tuple-element.7), channel_id=1, replica_groups=mesh['ra'=4,'cb'=4,'dp'=2] {'ra'}, use_global_device_ids=true, to_apply=%region_3.0 | all-reduce | flops 3072 | bytes 24576 | tf_op jit(solution)/shard_map/psum | solution.py:19
  38.3 0.0 copy-done.1
  38.3 0.0 copy-done.2
  38.3 4.6 add_convert_fusion.1
  42.9 0.0 all-gather.3.cloned.1.call-update
  42.9 0.0 all-gather.5.cloned.1.call-start
  42.9 12.3 %copy.17 = bf16[1024,4096]{0,1:T(8,128)(2,1)} copy(bf16[1024,4096]{1,0:T(8,128)(2,1)} %param.12) | data formatting | bytes 16777216 | tf_op args[4]
  55.2 373.1 %all_to_all.19 = bf16[1024,4,1024]{0,2,1:T(8,128)(2,1)} all-to-all(bf16[1024,4,1024]{0,2,1:T(8,128)(2,1)} %bitcast.10), channel_id=1, replica_groups=mesh['ra'=4,'cb'=4,'dp'=2] {'ra'}, dimensions={1} | all-to-all | bytes 16777216 | tf_op jit(solution)/shard_map/all_to_all | solution.py:23
  428.3 11.4 %copy.18 = bf16[4,1024,1024]{2,1,0:T(8,128)(2,1)} copy(bf16[4,1024,1024]{1,2,0:T(8,128)(2,1)} %bitcast.9) | data formatting | bytes 16777216 | tf_op jit(solution)/shard_map/all_to_all | solution.py:23
  439.6 0.0 all-gather.3.cloned.1.call-done
  439.6 19.2 %fusion.1 = bf16[1024,1536]{0,1:T(8,128)(2,1)} fusion(bf16[1536,4096]{0,1:T(8,128)(2,1)} %all-gather.3.cloned.1.call-done, bf16[4096,1024]{1,0:T(8,128)(2,1)} %bitcast.11), kind=kOutput, calls=%fused_computation.8 | convolution fusion | flops 12889620480 | bytes 24117248 | tf_op jit(solution)/shard_map/dot_general | solution.py:24
  458.9 0.0 all-gather.5.cloned.1.call-update
  458.9 217.1 %all-gather.5.cloned.1.call-done = bf16[4096,1536]{0,1:T(8,128)(2,1)} async-done(((bf16[1024,1536]{0,1:T(8,128)(2,1)}), bf16[4096,1536]{0,1:T(8,128)(2,1)}) %all-gather.5.cloned.1.call-update) | async-done | bytes 12582928 | tf_op jit(solution)/shard_map/all_gather | solution.py:32
  676.0 17.9 %fusion.3 = f32[1536,1024]{0,1:T(8,128)S(1)} fusion(bf16[4096,1536]{0,1:T(8,128)(2,1)} %all-gather.5.cloned.1.call-done, bf16[4096,1024]{1,0:T(8,128)(2,1)} %param.13), kind=kOutput, calls=%fused_computation.14 | convolution fusion | flops 12884901888 | bytes 27262976 | tf_op jit(solution)/shard_map/dot_general | solution.py:31
  694.0 0.0 copy-start
  694.0 1.5 collective-permute-start
  695.5 136.1 %collective-permute-done = f32[1536,1024]{0,1:T(8,128)} collective-permute-done((f32[1536,1024]{0,1:T(8,128)S(1)}, f32[1536,1024]{0,1:T(8,128)}, u32[]{:S(2)}, u32[]{:S(2)}) %collective-permute-start) | collective-permute-done | bytes 6291488 | tf_op jit(solution)/shard_map/ppermute | solution.py:39
  831.6 4.2 add.48
  835.8 0.0 copy-start.3
  835.8 0.0 copy-start.4
  835.8 1.5 collective-permute-start.1
  837.3 135.1 %collective-permute-done.1 = f32[1536,1024]{0,1:T(8,128)S(1)} collective-permute-done((f32[1536,1024]{0,1:T(8,128)S(1)}, f32[1536,1024]{0,1:T(8,128)S(1)}, u32[]{:S(2)}, u32[]{:S(2)}) %collective-permute-start.1) | collective-permute-done | bytes 6291488 | tf_op jit(solution)/shard_map/ppermute | solution.py:39
  972.4 0.0 copy-done
  972.4 3.7 fusion.2
  976.1 15.7 %all-reduce = (f32[1536]{0:T(1024)S(1)}, f32[1536]{0:T(1024)S(1)}) all-reduce(f32[1536]{0:T(1024)S(1)} %get-tuple-element.6, f32[1536]{0:T(1024)S(1)} %get-tuple-element.5), channel_id=1, replica_groups=mesh['ra'=4,'cb'=4,'dp'=2] {'ra'}, use_global_device_ids=true, to_apply=%region_7.0 | all-reduce | flops 3072 | bytes 24576 | tf_op jit(solution)/shard_map/psum | solution.py:43
  991.8 0.0 copy-done.3
  991.8 0.0 copy-done.4
  991.8 3.5 add_convert_fusion
  995.3 2.9 copy.19
  (2 shorter events, 0.0 us)
Async XLA Ops:
  6.5 433.1 %all-gather.3.cloned.1.call-start = ((), (), s32[]{:S(2)}) async-start(), calls=%async_computation.1 | async-start | bytes 15728640 | tf_op jit(solution)/shard_map/all_gather | solution.py:26
  9.7 28.5 %copy-start.1 = (f32[1024]{0:T(1024)S(1)}, f32[1024]{0:T(1024)}, u32[]{:S(2)}) copy-start(f32[1024]{0:T(1024)} %param.11) | copy-start | bytes 12292
  9.7 28.5 %copy-start.2 = (f32[1024]{0:T(1024)S(1)}, f32[1024]{0:T(1024)}, u32[]{:S(2)}) copy-start(f32[1024]{0:T(1024)} %param.10) | copy-start | bytes 12292
  42.9 633.1 %all-gather.5.cloned.1.call-start = ((), (), s32[]{:S(2)}) async-start(), calls=%async_computation.2 | async-start | bytes 15728640 | tf_op jit(solution)/shard_map/all_gather | solution.py:32
  694.0 278.4 %copy-start = (bf16[1536,1024]{0,1:T(8,128)(2,1)S(1)}, bf16[1536,1024]{0,1:T(8,128)(2,1)}, u32[]{:S(2)}) copy-start(bf16[1536,1024]{0,1:T(8,128)(2,1)} %add_convert_fusion.1) | copy-start | bytes 9437188
  694.0 137.6 %collective-permute-start = (f32[1536,1024]{0,1:T(8,128)S(1)}, f32[1536,1024]{0,1:T(8,128)}, u32[]{:S(2)}, u32[]{:S(2)}) collective-permute-start(f32[1536,1024]{0,1:T(8,128)S(1)} %fusion.3), channel_id=1, source_target_pairs={{0,2},{2,0},{4,6},{6,4},{1,3},{3,1},{5,7},{7,5},{8,10},{10,8},{12,... | collective-permute-start | bytes 18874376 | tf_op jit(solution)/shard_map/ppermute | solution.py:39
  835.8 156.0 %copy-start.3 = (f32[1024]{0:T(1024)S(1)}, f32[1024]{0:T(1024)}, u32[]{:S(2)}) copy-start(f32[1024]{0:T(1024)} %param.15) | copy-start | bytes 12292
  835.8 156.0 %copy-start.4 = (f32[1024]{0:T(1024)S(1)}, f32[1024]{0:T(1024)}, u32[]{:S(2)}) copy-start(f32[1024]{0:T(1024)} %param.14) | copy-start | bytes 12292
  835.8 136.6 %collective-permute-start.1 = (f32[1536,1024]{0,1:T(8,128)S(1)}, f32[1536,1024]{0,1:T(8,128)S(1)}, u32[]{:S(2)}, u32[]{:S(2)}) collective-permute-start(f32[1536,1024]{0,1:T(8,128)S(1)} %add.48), channel_id=1, source_target_pairs={{0,4},{2,6},{4,0},{6,2},{1,5},{3,7},{5,1},{7,3},{8,12},{10,14},{12... | collective-permute-start | bytes 18874376 | tf_op jit(solution)/shard_map/ppermute | solution.py:39
Sparse Core Ops, SparseCore 0:
  43.0 395.6 all-gather.2
  459.0 216.9 all-gather.4
